TPU v7x, 512 devices: a whole 4x8x8 slice. The times are simulated.
512 devices in a mesh: rep: 2 (over z_hi), fs: 32 (over z_lo, y), tp: 8 (over x, core).
Axes of the slice: x: 4, y: 8, z: 8 (z_hi: 2, z_lo: 4; z = z_hi * 4 + z_lo), core: 2. Of those that a mesh axis runs over, the one named last changes fastest.
Arguments:
- x_later: bfloat16 [8192, 2048], P(('rep', 'fs')), may hold values from -6 to 6
- kept_input_rows: bfloat16 [8192, 2048], P(('rep', 'fs')), may hold values from -6 to 6
- cotangent: bfloat16 [8192, 2048], P(('rep', 'fs')), may hold values from -8 to 8
- norm_gain_vector: float32 [2048], replicated, may hold values from 0.1 to 1.9
- up_weight: bfloat16 [2048, 4096], P('fs', 'tp'), may hold values from -0.125 to 0.125
- down_weight: bfloat16 [4096, 2048], P('tp', 'fs'), may hold values from -0.09375 to 0.09375
- up_sum: float32 [2048, 4096], P('fs', 'tp'), may hold values from -6 to 6
- down_sum: float32 [4096, 2048], P('tp', 'fs'), may hold values from -6 to 6
Outputs:
- mixed: bfloat16 [8192, 2048], P(('rep', 'fs'))
- input_gradient_rows: bfloat16 [8192, 2048], P(('rep', 'fs'))
- up_total: float32 [2048, 4096], P('fs', 'tp')
- down_total: float32 [4096, 2048], P('tp', 'fs')
All inputs are finite; a program needn't handle non-finite values.
Results may differ from a plain program's by a relative error of at most 0.018.
Values may be sent and summed in bfloat16 or wider, within the bound.
No kernel may reach another device: no remote copies, remote signals or barrier semaphores. Data moves between devices by JAX's collectives and lax.ppermute only.
A program may use at most 64 MiB of HBM per device.

v0:
```python
import jax
import jax.numpy as jnp
from jax import lax
from jax.sharding import Mesh
from jax.sharding import PartitionSpec as P

FS = ("fs_0", "fs_1")
REP_FS = ("rep", "fs_0", "fs_1")


EPSILON = 1e-06
TRANSPOSED = (((1,), (1,)), ((), ()))
LEADING = (((0,), (0,)), ((), ()))


def sent_to_all(shard, axis):
    copies = jnp.broadcast_to(shard, (lax.axis_size(axis), *shard.shape))
    return lax.all_to_all(copies, axis, split_axis=0, concat_axis=0, tiled=True)


def in_order(tiles, dim):
    lengths = list(tiles.shape[1:])
    lengths[dim] *= tiles.shape[0]
    return jnp.moveaxis(tiles, 0, dim).reshape(lengths)


def gathered_copies(shard, axis, dim):
    tiles = sent_to_all(shard, axis)
    return in_order(tiles, dim)


def together(arrays, axis):
    ends = [0]
    for a in arrays:
        ends.append(ends[-1] + a.size)
    subtotal = lax.psum(jnp.concatenate([a.ravel() for a in arrays]), axis)
    return tuple((subtotal[b:e].reshape(a.shape) for a, b, e in zip(arrays, ends, ends[1:])))


def all_blocks(shard, axes, order):
    tiles = shard[None]
    for k in order:
        tiles = lax.all_gather(tiles, axes[k], axis=0, tiled=True)
    held = [lax.axis_size(axes[k]) for k in reversed(order)]
    tiles = tiles.reshape(*held, *shard.shape)
    turned = sorted(range(len(order)), key=lambda place: order[len(order) - 1 - place])
    return tiles.transpose(*turned, *range(len(order), tiles.ndim)).reshape(-1, *shard.shape)


def gathered_by_axis(shard, axes, order, dim):
    return in_order(all_blocks(shard, axes, order), dim)


def over_copies(shard, axis):
    return sent_to_all(shard, axis).astype(jnp.float32).sum(axis=0)


def norm_partial_terms(values, norm_gain_vector):
    floats = values.astype(jnp.float32)
    inverse = lax.rsqrt(jnp.mean(floats * floats, axis=-1, keepdims=True) + EPSILON)
    unit_rows = floats * inverse
    normed = (unit_rows * norm_gain_vector).astype(jnp.bfloat16)
    return (inverse, unit_rows, normed)


def squared_relu(pre_act):
    return jnp.square(jax.nn.relu(pre_act)).astype(jnp.bfloat16)


def body(
    x_later, kept_input_rows, cotangent, norm_gain_vector, up_weight, down_weight, up_sum, down_sum
):
    row_count = x_later.shape[0]
    grad_scale = float(row_count * lax.axis_size("rep") * lax.axis_size(FS)) ** (-0.5)
    inv_later, unit_later, normed_later = norm_partial_terms(x_later, norm_gain_vector)
    inverse_rms_kept, unit_kept_rows, normed_kept_rows = norm_partial_terms(
        kept_input_rows, norm_gain_vector
    )
    stacked = jnp.concatenate([normed_kept_rows, normed_later], axis=0)
    columns = stacked
    pre_act = jnp.dot(
        columns, gathered_copies(up_weight, FS, 0), preferred_element_type=jnp.float32
    )
    pre_saved = pre_act[:row_count]
    hidden_saved = squared_relu(pre_saved)
    hidden_later = squared_relu(pre_act[row_count:])
    shard_part = gathered_copies(down_weight, FS, 1)
    product = jnp.dot(hidden_later, shard_part, preferred_element_type=jnp.float32)
    columns = cotangent
    grad_acc = lax.dot_general(columns, shard_part, TRANSPOSED, preferred_element_type=jnp.float32)
    pre_grad = (grad_acc * 2.0 * jax.nn.relu(pre_saved)).astype(jnp.bfloat16)
    back_part = lax.dot_general(
        pre_grad, gathered_copies(up_weight, FS, 0), TRANSPOSED, preferred_element_type=jnp.float32
    )
    mixed_sum, back_sum = tuple(
        (
            part.astype(jnp.float32)
            for part in together(
                (product.astype(jnp.bfloat16), back_part.astype(jnp.bfloat16)), "tp"
            )
        )
    )
    mixed = mixed_sum.astype(jnp.bfloat16)
    scaled_rows = back_sum * norm_gain_vector
    input_gradient_rows = (
        inverse_rms_kept
        * (
            scaled_rows
            - unit_kept_rows * jnp.mean(scaled_rows * unit_kept_rows, axis=-1, keepdims=True)
        )
    ).astype(jnp.bfloat16)
    cot_columns, normed_columns = (
        lax.all_to_all(cotangent, FS, split_axis=1, concat_axis=0, tiled=True),
        lax.all_to_all(normed_kept_rows, FS, split_axis=1, concat_axis=0, tiled=True),
    )
    columns = normed_columns
    up_grad = grad_scale * lax.dot_general(
        columns,
        gathered_by_axis(pre_grad, FS, (0, 1), 0),
        LEADING,
        preferred_element_type=jnp.float32,
    )
    columns = cot_columns
    down_grad = lax.dot_general(
        gathered_by_axis(hidden_saved, FS, (0, 1), 0),
        columns,
        LEADING,
        preferred_element_type=jnp.float32,
    )
    up_added, down_added = (
        over_copies(up_grad.astype(jnp.bfloat16), "rep").astype(jnp.float32),
        over_copies((down_grad * grad_scale).astype(jnp.bfloat16), "rep").astype(jnp.float32),
    )
    return (mixed, input_gradient_rows, up_sum + up_added, down_sum + down_added)


def solution(mesh):
    finer = Mesh(
        mesh.devices.reshape(mesh.shape["rep"], 4, 8, mesh.shape["tp"]),
        ("rep", "fs_0", "fs_1", "tp"),
    )
    return jax.shard_map(
        body,
        mesh=finer,
        in_specs=(
            P(REP_FS, None),
            P(REP_FS, None),
            P(REP_FS, None),
            P(),
            P(FS, "tp"),
            P("tp", FS),
            P(FS, "tp"),
            P("tp", FS),
        ),
        out_specs=(P(REP_FS, None), P(REP_FS, None), P(FS, "tp"), P("tp", FS)),
        check_vma=False,
    )
```

profile of v0, /device:TPU:2, one launch (start us, length us, event | category | flops | bytes accessed | tf_op | source)
XLA Modules:
  0.0 325.3 jit_solution(14748956280166571231)
XLA Ops:
  8.0 1.1 broadcast_in_dim.12
  9.1 0.0 copy-start.15
  9.1 64.7 %all_to_all.59 = bf16[32,64,512]{2,1,0:T(8,128)(2,1)} all-to-all(bf16[32,64,512]{2,1,0:T(8,128)(2,1)S(1)} %broadcast_in_dim.12), channel_id=1, replica_groups=mesh['rep'=2,'fs_0'=4,'fs_1'=8,'tp'=8] {'fs_0','fs_1'}, dimensions={0} | all-to-all | bytes 4194304 | tf_op jit(solution)/shard_map/all_to_all | solution.py:18
  73.8 0.0 copy-done.15
  73.8 1.5 broadcast_in_dim.26
  75.3 4.5 %all-to-all-start.1 = ((bf16[32,512,64]{1,2,0:T(8,128)(2,1)}), bf16[32,512,64]{1,2,0:T(8,128)(2,1)S(1)}, u32[]{:S(2)}, u32[]{:S(2)}) async-start(bf16[32,512,64]{1,2,0:T(8,128)(2,1)} %broadcast_in_dim.26), calls=%async_computation.1 | async-start | bytes 4194304 | tf_op jit(solution)/shard_map/all_to_all | solution.py:18
  79.8 0.0 all-reduce.2.cloned.1.call-start
  79.9 0.2 fusion.14
  80.1 0.2 fusion.15
  80.3 0.3 fusion.9
  80.6 0.0 copy-start.8
  80.6 0.8 copy-done.8
  81.4 0.1 copy-done.1
  81.5 1.5 fusion.18
  83.0 51.5 %all-to-all-done.1 = bf16[32,512,64]{1,2,0:T(8,128)(2,1)S(1)} async-done(((bf16[32,512,64]{1,2,0:T(8,128)(2,1)}), bf16[32,512,64]{1,2,0:T(8,128)(2,1)S(1)}, u32[]{:S(2)}, u32[]{:S(2)}) %all-to-all-start.1) | async-done | bytes 2097184 | tf_op jit(solution)/shard_map/all_to_all | solution.py:18
  134.5 1.8 fusion.3
  136.4 0.5 fusion.6
  136.8 1.1 copy-done.2
  137.9 0.8 fusion.4
  138.8 0.1 copy.43
  138.9 0.1 copy.42
  139.0 0.0 copy-start.9
  139.0 1.1 pad_maximum_fusion
  140.1 0.0 all-reduce.2.cloned.1.call-update
  140.1 0.0 copy-start.11
  140.1 0.0 all-gather.5.cloned.1.call-start
  140.2 15.7 %all-gather = bf16[512,512]{1,0:T(8,128)(2,1)} all-gather(bf16[128,512]{1,0:T(8,128)(2,1)S(1)} %fusion.6), channel_id=2, replica_groups=mesh['rep'=2,'fs_0'=4,'fs_1'=8,'tp'=8] {'fs_0'}, dimensions={0}, use_global_device_ids=true | all-gather | bytes 655360 | tf_op jit(solution)/shard_map/all_gather | solution.py:43
  155.9 0.0 all-gather.5.cloned.1.call-update
  155.9 1.0 copy.34
  156.9 5.6 %all-to-all-start.2 = ((bf16[128,32,64]{0,2,1:T(8,128)(2,1)}), bf16[128,32,64]{0,2,1:T(8,128)(2,1)S(1)}, u32[]{:S(2)}, u32[]{:S(2)}) async-start(bf16[128,32,64]{0,2,1:T(8,128)(2,1)} %bitcast.4), calls=%async_computation.2 | async-start | bytes 1048576 | tf_op jit(solution)/shard_map/all_to_all | solution.py:114
  162.5 0.0 all-gather.7.cloned.1.call-start
  162.5 0.0 copy-done.7
  162.5 1.0 copy.38
  163.6 21.1 %all-gather.1 = bf16[512,512]{1,0:T(8,128)(2,1)} all-gather(bf16[128,512]{1,0:T(8,128)(2,1)S(1)} %multiply_convert_fusion), channel_id=3, replica_groups=mesh['rep'=2,'fs_0'=4,'fs_1'=8,'tp'=8] {'fs_0'}, dimensions={0}, use_global_device_ids=true | all-gather | bytes 655360 | tf_op jit(solution)/shard_map/all_gather | solution.py:43
  184.7 0.0 all-gather.7.cloned.1.call-update
  184.8 0.0 all-to-all-done.2
  184.8 8.8 %all-to-all-start.4 = ((bf16[128,32,64]{0,2,1:T(8,128)(2,1)}), bf16[128,32,64]{0,2,1:T(8,128)(2,1)}, u32[]{:S(2)}, u32[]{:S(2)}) async-start(bf16[128,32,64]{0,2,1:T(8,128)(2,1)} %bitcast.14), calls=%async_computation.4 | async-start | bytes 1048576 | tf_op jit(solution)/shard_map/all_to_all | solution.py:113
  193.5 16.0 %all-reduce.2.cloned.1.call-done = bf16[524288]{0:T(1024)(128)(2,1)} async-done(((bf16[524288]{0:T(1024)(128)(2,1)}), bf16[524288]{0:T(1024)(128)(2,1)}) %all-reduce.2.cloned.1.call-update) | async-done | bytes 1048592 | tf_op jit(solution)/shard_map/psum | solution.py:36
  209.6 2.1 slice_convert_fusion
  211.7 0.2 reshape.80
  211.8 0.3 fusion.10
  212.1 12.9 %all-gather.5.cloned.1.call-done = bf16[32,128,512]{2,1,0:T(8,128)(2,1)} async-done(((bf16[4,128,512]{2,1,0:T(8,128)(2,1)}), bf16[32,128,512]{2,1,0:T(8,128)(2,1)}) %all-gather.5.cloned.1.call-update) | async-done | bytes 4194320 | tf_op jit(solution)/shard_map/all_gather | solution.py:43
  225.0 4.6 %copy.36 = bf16[4,8,128,512]{3,2,1,0:T(8,128)(2,1)} copy(bf16[4,8,128,512]{3,2,0,1:T(8,128)(2,1)} %bitcast.52) | data formatting | bytes 8388608 | tf_op jit(solution)/shard_map/transpose | solution.py:47
  229.6 53.1 %all-gather.7.cloned.1.call-done = bf16[32,128,512]{2,1,0:T(8,128)(2,1)} async-done(((bf16[4,128,512]{2,1,0:T(8,128)(2,1)}), bf16[32,128,512]{2,1,0:T(8,128)(2,1)}) %all-gather.7.cloned.1.call-update) | async-done | bytes 4194320 | tf_op jit(solution)/shard_map/all_gather | solution.py:43
  282.8 4.7 %copy.37 = bf16[4,8,128,512]{3,2,1,0:T(8,128)(2,1)} copy(bf16[4,8,128,512]{3,2,0,1:T(8,128)(2,1)} %bitcast.53) | data formatting | bytes 8388608 | tf_op jit(solution)/shard_map/transpose | solution.py:47
  287.5 0.0 copy-done
  287.5 0.8 fusion.7
  288.3 0.0 all-to-all-done.4
  288.3 0.7 broadcast_in_dim.28
  289.0 7.4 %all-to-all-start.3 = ((bf16[2,64,512]{2,1,0:T(8,128)(2,1)}), bf16[2,64,512]{2,1,0:T(8,128)(2,1)S(1)}, u32[]{:S(2)}, u32[]{:S(2)}) async-start(bf16[2,64,512]{2,1,0:T(8,128)(2,1)} %broadcast_in_dim.28), calls=%async_computation.3 | async-start | bytes 262144 | tf_op jit(solution)/shard_map/all_to_all | solution.py:18
  296.4 3.2 fusion.8
  299.6 0.0 copy-start.4
  299.6 0.0 copy-start.12
  299.6 5.2 %all-to-all-done.3 = bf16[2,64,512]{2,1,0:T(8,128)(2,1)S(1)} async-done(((bf16[2,64,512]{2,1,0:T(8,128)(2,1)}), bf16[2,64,512]{2,1,0:T(8,128)(2,1)S(1)}, u32[]{:S(2)}, u32[]{:S(2)}) %all-to-all-start.3) | async-done | bytes 131104 | tf_op jit(solution)/shard_map/all_to_all | solution.py:18
  304.8 0.7 broadcast_in_dim.30
  305.4 3.4 %all-to-all-start.5 = ((bf16[2,512,64]{1,2,0:T(8,128)(2,1)}), bf16[2,512,64]{1,2,0:T(8,128)(2,1)S(1)}, u32[]{:S(2)}, u32[]{:S(2)}) async-start(bf16[2,512,64]{1,2,0:T(8,128)(2,1)} %broadcast_in_dim.30), calls=%async_computation.5 | async-start | bytes 262144 | tf_op jit(solution)/shard_map/all_to_all | solution.py:18
  308.8 0.0 copy-start.13
  308.8 1.1 fusion.13
  310.0 0.0 copy-done.4
  310.0 1.0 slice.33
  311.0 0.0 copy-done.12
  311.0 0.7 add.26
  311.7 5.5 %all-to-all-done.5 = bf16[2,512,64]{1,2,0:T(8,128)(2,1)S(1)} async-done(((bf16[2,512,64]{1,2,0:T(8,128)(2,1)}), bf16[2,512,64]{1,2,0:T(8,128)(2,1)S(1)}, u32[]{:S(2)}, u32[]{:S(2)}) %all-to-all-start.5) | async-done | bytes 131104 | tf_op jit(solution)/shard_map/all_to_all | solution.py:18
  317.2 0.7 add.27
  (22 shorter events, 0.1 us)
Async XLA Ops:
  9.1 64.7 %copy-start.15 = (bf16[512,64]{0,1:T(8,128)(2,1)S(1)}, bf16[512,64]{0,1:T(8,128)(2,1)}, u32[]{:S(2)}) copy-start(bf16[512,64]{0,1:T(8,128)(2,1)} %param.13) | copy-start | bytes 196612
  75.3 4.6 %copy-start.3 = (bf16[128,2048]{1,0:T(8,128)(2,1)S(1)}, bf16[128,2048]{1,0:T(8,128)(2,1)}, u32[]{:S(2)}) copy-start(bf16[128,2048]{1,0:T(8,128)(2,1)} %param.9) | copy-start | bytes 1572868
  75.3 4.8 %copy-start.5 = (bf16[128,2048]{1,0:T(8,128)(2,1)S(1)}, bf16[128,2048]{1,0:T(8,128)(2,1)}, u32[]{:S(2)}) copy-start(bf16[128,2048]{1,0:T(8,128)(2,1)} %param.8) | copy-start | bytes 1572868
  75.3 5.0 %copy-start.14 = (f32[2048]{0:T(1024)S(1)}, f32[2048]{0:T(1024)}, u32[]{:S(2)}) copy-start(f32[2048]{0:T(1024)} %param.11) | copy-start | bytes 24580
  75.3 59.2 %all-to-all-start.1 = ((bf16[32,512,64]{1,2,0:T(8,128)(2,1)}), bf16[32,512,64]{1,2,0:T(8,128)(2,1)S(1)}, u32[]{:S(2)}, u32[]{:S(2)}) async-start(bf16[32,512,64]{1,2,0:T(8,128)(2,1)} %broadcast_in_dim.26), calls=%async_computation.1 | async-start | bytes 4194304 | tf_op jit(solution)/shard_map/all_to_all | solution.py:18
  79.8 129.7 %all-reduce.2.cloned.1.call-start = ((), (), s32[]{:S(2)}) async-start(), calls=%async_computation.6 | async-start | bytes 2097152 | tf_op jit(solution)/shard_map/psum | solution.py:36
  79.9 1.6 copy-start.1
  80.6 0.8 copy-start.8
  83.0 53.4 %copy-start.6 = (bf16[128,2048]{1,0:T(8,128)(2,1)S(1)}, bf16[128,2048]{1,0:T(8,128)(2,1)}, u32[]{:S(2)}) copy-start(bf16[128,2048]{1,0:T(8,128)(2,1)} %param.10) | copy-start | bytes 1572868
  134.5 1.9 copy-start.10
  136.3 1.6 copy-start.2
  139.0 16.9 %copy-start.9 = (bf16[128,2048]{1,0:T(8,128)(2,1)S(1)}, bf16[128,2048]{1,0:T(8,128)(2,1)}, u32[]{:S(2)}) copy-start(bf16[128,2048]{1,0:T(8,128)(2,1)} %copy-done.8) | copy-start | bytes 1572868
  140.1 22.5 %copy-start.7 = (bf16[128,2048]{1,0:T(8,128)(2,1)S(1)}, bf16[128,2048]{1,0:T(8,128)(2,1)}, u32[]{:S(2)}) copy-start(bf16[128,2048]{1,0:T(8,128)(2,1)} %param.10) | copy-start | bytes 1572868
  140.1 23.5 %copy-start.11 = (f32[256,512]{1,0:T(8,128)S(1)}, f32[256,512]{1,0:T(8,128)}, u32[]{:S(2)}) copy-start(f32[256,512]{1,0:T(8,128)} %fusion.18) | copy-start | bytes 1572868
  140.1 84.9 %all-gather.5.cloned.1.call-start = ((), (), s32[]{:S(2)}) async-start(), calls=%async_computation.7 | async-start | bytes 4718592 | tf_op jit(solution)/shard_map/all_gather | solution.py:43
  156.9 27.9 %all-to-all-start.2 = ((bf16[128,32,64]{0,2,1:T(8,128)(2,1)}), bf16[128,32,64]{0,2,1:T(8,128)(2,1)S(1)}, u32[]{:S(2)}, u32[]{:S(2)}) async-start(bf16[128,32,64]{0,2,1:T(8,128)(2,1)} %bitcast.4), calls=%async_computation.2 | async-start | bytes 1048576 | tf_op jit(solution)/shard_map/all_to_all | solution.py:114
  162.5 120.3 %all-gather.7.cloned.1.call-start = ((), (), s32[]{:S(2)}) async-start(), calls=%async_computation.8 | async-start | bytes 4718592 | tf_op jit(solution)/shard_map/all_gather | solution.py:43
  184.8 103.6 %all-to-all-start.4 = ((bf16[128,32,64]{0,2,1:T(8,128)(2,1)}), bf16[128,32,64]{0,2,1:T(8,128)(2,1)}, u32[]{:S(2)}, u32[]{:S(2)}) async-start(bf16[128,32,64]{0,2,1:T(8,128)(2,1)} %bitcast.14), calls=%async_computation.4 | async-start | bytes 1048576 | tf_op jit(solution)/shard_map/all_to_all | solution.py:113
  282.8 4.7 %copy-start = (bf16[4,8,128,512]{3,2,1,0:T(8,128)(2,1)S(1)}, bf16[4,8,128,512]{3,2,1,0:T(8,128)(2,1)}, u32[]{:S(2)}) copy-start(bf16[4,8,128,512]{3,2,1,0:T(8,128)(2,1)} %copy.36) | copy-start | bytes 12582916
  289.0 15.7 %all-to-all-start.3 = ((bf16[2,64,512]{2,1,0:T(8,128)(2,1)}), bf16[2,64,512]{2,1,0:T(8,128)(2,1)S(1)}, u32[]{:S(2)}, u32[]{:S(2)}) async-start(bf16[2,64,512]{2,1,0:T(8,128)(2,1)} %broadcast_in_dim.28), calls=%async_computation.3 | async-start | bytes 262144 | tf_op jit(solution)/shard_map/all_to_all | solution.py:18
  299.6 10.4 %copy-start.4 = (bf16[262144]{0:T(1024)(128)(2,1)S(1)}, bf16[262144]{0:T(1024)(128)(2,1)}, u32[]{:S(2)}) copy-start(bf16[262144]{0:T(1024)(128)(2,1)} %get-tuple-element.9) | copy-start | bytes 1572868
  299.6 11.4 %copy-start.12 = (f32[64,512]{1,0:T(8,128)S(1)}, f32[64,512]{1,0:T(8,128)}, u32[]{:S(2)}) copy-start(f32[64,512]{1,0:T(8,128)} %param.14) | copy-start | bytes 393220
  305.4 11.8 %all-to-all-start.5 = ((bf16[2,512,64]{1,2,0:T(8,128)(2,1)}), bf16[2,512,64]{1,2,0:T(8,128)(2,1)S(1)}, u32[]{:S(2)}, u32[]{:S(2)}) async-start(bf16[2,512,64]{1,2,0:T(8,128)(2,1)} %broadcast_in_dim.30), calls=%async_computation.5 | async-start | bytes 262144 | tf_op jit(solution)/shard_map/all_to_all | solution.py:18
  308.8 8.4 %copy-start.13 = (f32[512,64]{0,1:T(8,128)S(1)}, f32[512,64]{0,1:T(8,128)}, u32[]{:S(2)}) copy-start(f32[512,64]{0,1:T(8,128)} %param.15) | copy-start | bytes 393220
Sparse Core Ops, SparseCore 0:
  140.2 69.2 all-reduce.1
Sparse Core Ops, SparseCore 1:
  156.0 69.0 all-gather.4
  227.0 55.7 all-gather.6
where the time goes:
time: 326 us; the launch traced here: 325 us
  waiting for transfers between devices  144 us (44%)
  blocking collectives  101 us (31%)
  starting transfers between devices  29.7 us (9%)
  local copies, waits for them, and re-layouts  18.8 us (6%)
  between operations  15.8 us (5%)
  matrix products  8.61 us (3%)
  other arithmetic  6.7 us (2%)
    all_gather x2, waiting for transfers between devices, all_blocks(): tiles = lax.all_gather(tiles, axes[k], axis=0, tiled=True)  66 us
    all_to_all x1, blocking collectives, sent_to_all(): return lax.all_to_all(copies, axis, split_axis=0, concat_axis=0, tiled=True)  64.7 us
    all_to_all x3, waiting for transfers between devices, sent_to_all(): return lax.all_to_all(copies, axis, split_axis=0, concat_axis=0, tiled=True)  62.2 us
    all_gather x2, blocking collectives, all_blocks(): tiles = lax.all_gather(tiles, axes[k], axis=0, tiled=True)  36.8 us
    psum x1, waiting for transfers between devices, together(): subtotal = lax.psum(jnp.concatenate([a.ravel() for a in arrays]), axis)  16 us
    all_to_all x3, starting transfers between devices, sent_to_all(): return lax.all_to_all(copies, axis, split_axis=0, concat_axis=0, tiled=True)  15.2 us
    transpose x2, local copies, waits for them, and re-layouts, all_blocks(): tiles.transpose(*turned, *range(len(order), tiles.ndim))  9.32 us
    all_to_all x1, starting transfers between devices, body(): lax.all_to_all(cotangent, FS, split_axis=1, concat_axis=0, tiled=True)  8.76 us
  transfers between devices with their start and end apart: 8, of which 6 were waited for; matrix products, arithmetic and copies ran while one was open for 7% of the time, Pallas kernels for 0%

commit v1 on v0

v1 whole, which is shorter than its diff:
```python
import jax
import jax.numpy as jnp
from jax import lax
from jax.sharding import Mesh
from jax.sharding import PartitionSpec as P

FS = ("zl", "yh", "yl")
Y = ("yh", "yl")
Z = ("rep", "zl")
TP = ("x", "core")
ROWS = ("rep", "zl", "yh", "yl")

EPSILON = 1e-06
F32 = jnp.float32
BF16 = jnp.bfloat16
CONTRACT_LAST = (((1,), (1,)), ((), ()))
CONTRACT_FIRST = (((0,), (0,)), ((), ()))


def around(values, axes, step):
    count = lax.axis_size(axes)
    return lax.ppermute(values, axes, [(i, (i + step) % count) for i in range(count)])


def swapped(values, axis):
    return lax.ppermute(values, axis, [(0, 1), (1, 0)])


def exchanged(blocks, axes):
    return lax.all_to_all(blocks, axes, split_axis=0, concat_axis=0, tiled=True)


def norm_terms(values, gain):
    floats = values.astype(F32)
    inverse = lax.rsqrt(jnp.mean(floats * floats, axis=-1, keepdims=True) + EPSILON)
    unit = floats * inverse
    return inverse, unit, (unit * gain).astype(BF16)


def body(x_later, kept, cotangent, gain, up_weight, down_weight, up_sum, down_sum):
    rows, width = x_later.shape
    half = rows // 2
    depth, units = up_weight.shape
    own_units = units // 2
    n_y = lax.axis_size(Y)
    n_z = lax.axis_size("zl")
    n_x = lax.axis_size("x")
    grad_scale = float(rows * lax.axis_size("rep") * lax.axis_size(FS)) ** (-0.5)
    core = lax.axis_index("core")
    pair = lax.axis_index("yl")
    z = lax.axis_index("zl")

    both = jnp.stack([up_weight, down_weight.T])
    halves = both.reshape(2, depth, 2, own_units).transpose(2, 0, 1, 3)
    copies = jnp.broadcast_to(halves[None], (n_y // 2, *halves.shape)).reshape(n_y, 2, depth, own_units)
    held = exchanged(copies, Y)

    def split_rows(a):
        mine = lax.dynamic_slice_in_dim(a, core * half, half, 0)
        other = lax.dynamic_slice_in_dim(a, (1 - core) * half, half, 0)
        return mine, other

    own = [split_rows(a) for a in (kept, x_later, cotangent)]
    partner_mine = swapped(jnp.stack([mine for mine, _ in own]), "yl")

    w_next = around(held, Z, 1)
    w_prev = around(held, Z, -1)
    w_far_low = around(held[: n_y // 2], Z, 2)
    w_far_high = around(held[n_y // 2 :], Z, -2)

    partner_other = swapped(partner_mine, "core")
    kept_rows, later_rows, cot_rows = (
        jnp.concatenate([own[i][0], own[i][1], partner_mine[i], partner_other[i]], axis=0)
        for i in range(3)
    )
    inverse, unit, normed_saved = norm_terms(kept_rows, gain)
    _, _, normed_later = norm_terms(later_rows, gain)

    weights = jnp.zeros((2, n_z, n_y, depth, own_units), BF16)

    def placed(weights, piece, at, first=0):
        block = piece.transpose(1, 0, 2, 3)[:, None]
        return lax.dynamic_update_slice(weights, block, (0, lax.rem(at, n_z), first, 0, 0))

    weights = placed(weights, held, z)
    weights = placed(weights, w_next, z + n_z - 1)
    weights = placed(weights, w_prev, z + 1)
    weights = placed(weights, w_far_low, z + 2)
    weights = placed(weights, w_far_high, z + 2, n_y // 2)
    up_all = weights[0].reshape(width, own_units)
    down_all = weights[1].reshape(width, own_units)

    pre = jnp.dot(
        jnp.concatenate([normed_saved, normed_later]), up_all, preferred_element_type=F32
    )
    pre_saved = jax.nn.relu(pre[: 2 * rows])
    pre_later = jax.nn.relu(pre[2 * rows :])
    hidden_saved = jnp.square(pre_saved).astype(BF16)
    hidden_later = jnp.square(pre_later).astype(BF16)
    hidden_grad = jnp.dot(cot_rows, down_all, preferred_element_type=F32)
    pre_grad = (hidden_grad * 2.0 * pre_saved).astype(BF16)

    up_part = lax.dot_general(normed_saved, pre_grad, CONTRACT_FIRST, preferred_element_type=F32)
    down_part = lax.dot_general(cot_rows, hidden_saved, CONTRACT_FIRST, preferred_element_type=F32)
    parts = jnp.stack([up_part, down_part]).reshape(2, n_z, n_y, depth, own_units)

    def block_of(at):
        return lax.dynamic_index_in_dim(parts, lax.rem(at, n_z), 1, keepdims=False)

    far = block_of(z + 2).astype(BF16)
    g_next = around(block_of(z + 1).astype(BF16), Z, 1)
    g_prev = around(block_of(z + n_z - 1).astype(BF16), Z, -1)
    g_far_low = around(far[:, : n_y // 2], Z, 2)
    g_far_high = around(far[:, n_y // 2 :], Z, -2)

    mixed_part = lax.dot_general(hidden_later, down_all, CONTRACT_LAST, preferred_element_type=F32)
    back_part = lax.dot_general(pre_grad, up_all, CONTRACT_LAST, preferred_element_type=F32)
    outs = jnp.stack([mixed_part, back_part]).reshape(2, 2, 2, half, width)
    from_core = swapped(outs[:, :, 1].astype(BF16), "core")
    core_sum = outs[:, :, 0] + from_core.astype(F32)
    first = jnp.where(pair == 0, core_sum[:, 0], core_sum[:, 1])
    second = jnp.where(pair == 0, core_sum[:, 1], core_sum[:, 0])
    columns = width // n_x
    sends = jnp.stack([first, second]).astype(BF16).reshape(2, 2, half, n_x, columns)
    sends = sends.transpose(0, 3, 1, 2, 4).reshape(2 * n_x, 2, half, columns)
    summed = exchanged(sends, ("yl", "x")).astype(F32).sum(axis=0).astype(BF16)

    block = block_of(z)
    far_sum = jnp.concatenate([g_far_low, g_far_high], axis=1)
    block = block + g_next.astype(F32) + g_prev.astype(F32) + far_sum.astype(F32)
    over_y = exchanged(block.astype(BF16).transpose(1, 0, 2, 3), Y).astype(F32)
    shard = over_y.reshape(n_y // 2, 2, 2, depth, own_units).sum(axis=0)
    shard = (shard * grad_scale).astype(BF16)
    other_rep = swapped(shard, "rep")

    gathered = exchanged(jnp.broadcast_to(summed[None], (n_x, *summed.shape)), "x")
    gathered = gathered.transpose(1, 2, 0, 3).reshape(2, half, width)
    scaled = gathered[1].astype(F32) * gain
    unit_mine = unit[:half]
    input_grad = inverse[:half] * (
        scaled - unit_mine * jnp.mean(scaled * unit_mine, axis=-1, keepdims=True)
    )
    mine = jnp.stack([gathered[0], input_grad.astype(BF16)])
    theirs = swapped(mine, "core")
    mixed, input_gradient_rows = (
        jnp.concatenate(
            [jnp.where(core == 0, mine[i], theirs[i]), jnp.where(core == 0, theirs[i], mine[i])]
        )
        for i in range(2)
    )

    total = (shard.astype(F32) + other_rep.astype(F32)).transpose(1, 2, 0, 3)
    total = total.reshape(2, depth, units)
    return mixed, input_gradient_rows, up_sum + total[0], down_sum + total[1].T


def solution(mesh):
    finer = Mesh(
        mesh.devices.reshape(mesh.shape["rep"], 4, 4, 2, 4, 2),
        ("rep", "zl", "yh", "yl", "x", "core"),
    )
    return jax.shard_map(
        body,
        mesh=finer,
        in_specs=(
            P(ROWS, None),
            P(ROWS, None),
            P(ROWS, None),
            P(),
            P(FS, TP),
            P(TP, FS),
            P(FS, TP),
            P(TP, FS),
        ),
        out_specs=(P(ROWS, None), P(ROWS, None), P(FS, TP), P(TP, FS)),
        check_vma=False,
    )
```

time: 326 us -> 182 us (0.56)
  blocking collectives: 101 us -> 0 us
  waiting for transfers between devices: 144 us -> 79.4 us
  starting transfers between devices: 29.7 us -> 73.9 us
  between operations: 15.8 us -> 1.35 us
  local copies, waits for them, and re-layouts: 18.8 us -> 8.04 us
  other arithmetic: 6.7 us -> 14.6 us
  matrix products: 8.61 us -> 4.02 us
    all_gather x2 -> x0, waiting for transfers between devices: 66 us -> none  [all_blocks(): tiles = lax.all_gather(tiles, axes[k], axis=0, tiled=True)]
    all_to_all x1 -> x0, blocking collectives: 64.7 us -> none  [sent_to_all(): return lax.all_to_all(copies, axis, split_axis=0, concat_axis=0, tiled=True)]
    ppermute x0 -> x13, waiting for transfers between devices: none -> 62 us  [the longest x8 31.6 us: around(): lax.ppermute(values, axes, [(i, (i + step) % count) for i in range(count)])]
    ppermute x0 -> x13, starting transfers between devices: none -> 50.5 us  [the longest x8 35.8 us: around(): lax.ppermute(values, axes, [(i, (i + step) % count) for i in range(count)])]
    all_to_all x5 -> x4, waiting for transfers between devices: 62.2 us -> 17.4 us  [exchanged(): return lax.all_to_all(blocks, axes, split_axis=0, concat_axis=0, tiled=True)]
    all_gather x2 -> x0, blocking collectives: 36.8 us -> none  [all_blocks(): tiles = lax.all_gather(tiles, axes[k], axis=0, tiled=True)]
    psum x1 -> x0, waiting for transfers between devices: 16 us -> none  [together(): subtotal = lax.psum(jnp.concatenate([a.ravel() for a in arrays]), axis)]
    transpose x2 -> x1, local copies, waits for them, and re-layouts: 9.32 us -> 0.02 us  [body(): halves = both.reshape(2, depth, 2, own_units).transpose(2, 0, 1, 3)]
  transfers between devices with their start and end apart: 8 -> 17, of which waited for: 6 -> 10; matrix products, arithmetic and copies ran while one was open for 7% -> 5% of each run, Pallas kernels for 0% -> 0%
where the time goes in v1:
time: 182 us; the launch traced here: 181 us
  waiting for transfers between devices  79.4 us (44%)
  starting transfers between devices  73.9 us (41%)
  other arithmetic  14.6 us (8%)
  local copies, waits for them, and re-layouts  8.04 us (4%)
  matrix products  4.02 us (2%)
    ppermute x8, starting transfers between devices, around(): lax.ppermute(values, axes, [(i, (i + step) % count) for i in range(count)])  35.8 us
    ppermute x8, waiting for transfers between devices, around(): lax.ppermute(values, axes, [(i, (i + step) % count) for i in range(count)])  31.6 us
    ppermute x5, waiting for transfers between devices, swapped(): return lax.ppermute(values, axis, [(0, 1), (1, 0)])  30.4 us
    all_to_all x4, starting transfers between devices, exchanged(): return lax.all_to_all(blocks, axes, split_axis=0, concat_axis=0, tiled=True)  23.4 us
    all_to_all x4, waiting for transfers between devices, exchanged(): return lax.all_to_all(blocks, axes, split_axis=0, concat_axis=0, tiled=True)  17.4 us
    ppermute x5, starting transfers between devices, swapped(): return lax.ppermute(values, axis, [(0, 1), (1, 0)])  14.7 us
  transfers between devices with their start and end apart: 17, of which 10 were waited for; matrix products, arithmetic and copies ran while one was open for 5% of the time, Pallas kernels for 0%

profile of v1, /device:TPU:2, one launch (start us, length us, event | category | flops | bytes accessed | tf_op | source)
XLA Modules:
  0.0 181.3 jit_solution(121520279530532814)
XLA Ops:
  0.7 1.0 stack.51
  1.6 0.9 stack.52
  2.5 0.2 maximum_bitcast_fusion
  2.7 0.8 broadcast_in_dim.17
  3.6 7.1 %all-to-all-start = ((bf16[8,2,64,256]{3,2,1,0:T(8,128)(2,1)}), bf16[8,2,64,256]{3,2,1,0:T(8,128)(2,1)S(1)}, u32[]{:S(2)}, u32[]{:S(2)}) async-start(bf16[8,2,64,256]{3,2,1,0:T(8,128)(2,1)} %bitcast.9), calls=%async_computation | async-start | bytes 1048576 | tf_op jit(solution)/shard_map/all_to_all | solution.py:30
  10.7 0.8 constant_dynamic-slice_fusion
  11.6 1.0 pad_maximum_fusion.5
  12.6 3.9 %collective-permute-start = (bf16[3,64,2048]{2,1,0:T(8,128)(2,1)}, bf16[3,64,2048]{2,1,0:T(8,128)(2,1)S(1)}, u32[]{:S(2)}, u32[]{:S(2)}) collective-permute-start(bf16[3,64,2048]{2,1,0:T(8,128)(2,1)} %pad_maximum_fusion.5), channel_id=1, source_target_pairs={{0,8},{8,0},{1,9},{9,1},{2,10},{10,2},{3,11},{11,3},{4,12},{12,4},... | collective-permute-start | bytes 2359304 | tf_op jit(solution)/shard_map/ppermute | solution.py:26
  16.5 24.6 %collective-permute-done = bf16[3,64,2048]{2,1,0:T(8,128)(2,1)S(1)} collective-permute-done((bf16[3,64,2048]{2,1,0:T(8,128)(2,1)}, bf16[3,64,2048]{2,1,0:T(8,128)(2,1)S(1)}, u32[]{:S(2)}, u32[]{:S(2)}) %collective-permute-start) | collective-permute-done | bytes 786464 | tf_op jit(solution)/shard_map/ppermute | solution.py:26
  41.1 1.9 %collective-permute-start.1 = (bf16[3,64,2048]{2,1,0:T(8,128)(2,1)S(1)}, bf16[3,64,2048]{2,1,0:T(8,128)(2,1)}, u32[]{:S(2)}, u32[]{:S(2)}) collective-permute-start(bf16[3,64,2048]{2,1,0:T(8,128)(2,1)S(1)} %collective-permute-done), channel_id=1, source_target_pairs={{0,1},{1,0},{2,3},{3,2},{4,5},{5,4},{6,7},{7,6},{8,9},{9,8},{10,11... | collective-permute-start | bytes 2359304 | tf_op jit(solution)/shard_map/ppermute | solution.py:26
  43.0 4.3 %collective-permute-start.2 = (bf16[8,2,64,256]{3,2,1,0:T(8,128)(2,1)S(1)}, bf16[8,2,64,256]{3,2,1,0:T(8,128)(2,1)S(1)}, u32[]{:S(2)}, u32[]{:S(2)}) collective-permute-start(bf16[8,2,64,256]{3,2,1,0:T(8,128)(2,1)S(1)} %all-to-all-done), channel_id=1, source_target_pairs={{0,64},{64,128},{128,192},{192,256},{256,320},{320,384},{384,448},... | collective-permute-start | bytes 1572872 | tf_op jit(solution)/shard_map/ppermute | solution.py:22
  47.4 8.6 %collective-permute-start.3 = (bf16[8,2,64,256]{3,2,1,0:T(8,128)(2,1)S(1)}, bf16[8,2,64,256]{3,2,1,0:T(8,128)(2,1)S(1)}, u32[]{:S(2)}, u32[]{:S(2)}) collective-permute-start(bf16[8,2,64,256]{3,2,1,0:T(8,128)(2,1)S(1)} %all-to-all-done), channel_id=1, source_target_pairs={{0,448},{64,0},{128,64},{192,128},{256,192},{320,256},{384,320},{4... | collective-permute-start | bytes 1572872 | tf_op jit(solution)/shard_map/ppermute | solution.py:22
  56.0 1.9 %collective-permute-start.4 = (bf16[4,2,64,256]{3,2,1,0:T(8,128)(2,1)S(1)}, bf16[4,2,64,256]{3,2,1,0:T(8,128)(2,1)S(1)}, u32[]{:S(2)}, u32[]{:S(2)}) collective-permute-start(bf16[4,2,64,256]{3,2,1,0:T(8,128)(2,1)S(1)} %get-tuple-element.38), channel_id=1, source_target_pairs={{0,128},{64,192},{128,256},{192,320},{256,384},{320,448},{384,0},{... | collective-permute-start | bytes 786440 | tf_op jit(solution)/shard_map/ppermute | solution.py:22
  58.0 6.0 %collective-permute-start.5 = (bf16[4,2,64,256]{3,2,1,0:T(8,128)(2,1)S(1)}, bf16[4,2,64,256]{3,2,1,0:T(8,128)(2,1)S(1)}, u32[]{:S(2)}, u32[]{:S(2)}) collective-permute-start(bf16[4,2,64,256]{3,2,1,0:T(8,128)(2,1)S(1)} %get-tuple-element.37), channel_id=1, source_target_pairs={{0,384},{64,448},{128,0},{192,64},{256,128},{320,192},{384,256},{4... | collective-permute-start | bytes 786440 | tf_op jit(solution)/shard_map/ppermute | solution.py:22
  64.0 0.2 broadcast_in_dim.16
  64.3 2.4 %collective-permute-done.2 = bf16[8,2,64,256]{3,2,1,0:T(8,128)(2,1)S(1)} collective-permute-done((bf16[8,2,64,256]{3,2,1,0:T(8,128)(2,1)S(1)}, bf16[8,2,64,256]{3,2,1,0:T(8,128)(2,1)S(1)}, u32[]{:S(2)}, u32[]{:S(2)}) %collective-permute-start.2) | collective-permute-done | bytes 524320 | tf_op jit(solution)/shard_map/ppermute | solution.py:22
  66.8 7.1 %collective-permute-done.3 = bf16[8,2,64,256]{3,2,1,0:T(8,128)(2,1)S(1)} collective-permute-done((bf16[8,2,64,256]{3,2,1,0:T(8,128)(2,1)S(1)}, bf16[8,2,64,256]{3,2,1,0:T(8,128)(2,1)S(1)}, u32[]{:S(2)}, u32[]{:S(2)}) %collective-permute-start.3) | collective-permute-done | bytes 524320 | tf_op jit(solution)/shard_map/ppermute | solution.py:22
  74.0 5.0 %collective-permute-done.5 = bf16[4,2,64,256]{3,2,1,0:T(8,128)(2,1)S(1)} collective-permute-done((bf16[4,2,64,256]{3,2,1,0:T(8,128)(2,1)S(1)}, bf16[4,2,64,256]{3,2,1,0:T(8,128)(2,1)S(1)}, u32[]{:S(2)}, u32[]{:S(2)}) %collective-permute-start.5) | collective-permute-done | bytes 262176 | tf_op jit(solution)/shard_map/ppermute | solution.py:22
  79.1 0.2 fusion.47
  79.4 1.2 slice_bitcast_fusion.2
  80.5 0.3 fusion.1
  80.8 0.3 fusion
  81.2 3.3 %convert_multiply_fusion.2 = (f32[256,2048]{1,0:T(8,128)}, bf16[256,2048]{1,0:T(8,128)(2,1)S(1)}, bf16[256,2048]{1,0:T(8,128)(2,1)S(1)}) fusion(f32[256]{0:T(256)S(1)} %add_rsqrt_fusion.1, bf16[64,2048]{1,0:T(8,128)(2,1)S(1)} %get-tuple-element.23, bf16[64,2048]{1,0:T(8,128)(2,1)S(1)} %get-tuple-element.20, bf16[64,2048]{1,0:T(8,128)(2,1)S(1)} %get-tuple-element.33, ...), kind=kLoop, calls=%fused_computation.14 | loop fusion | flops 11534336 | bytes 6301696 | tf_op jit(solution)/shard_map/mul | solution.py:36
  84.4 0.7 fusion.8
  85.2 0.2 copy-done.3
  85.5 0.4 fusion.13
  85.9 0.5 convolution_bitcast_fusion
  86.4 0.5 convolution_bitcast_fusion.1
  86.9 1.3 fusion.14
  88.2 0.3 copy-done
  88.5 1.9 %collective-permute-start.6 = (bf16[2,2,64,2048]{3,2,1,0:T(8,128)(2,1)}, bf16[2,2,64,2048]{3,2,1,0:T(8,128)(2,1)}, u32[]{:S(2)}, u32[]{:S(2)}) collective-permute-start(bf16[2,2,64,2048]{3,2,1,0:T(8,128)(2,1)} %fusion.14), channel_id=1, source_target_pairs={{0,1},{1,0},{2,3},{3,2},{4,5},{5,4},{6,7},{7,6},{8,9},{9,8},{10,11... | collective-permute-start | bytes 3145736 | tf_op jit(solution)/shard_map/ppermute | solution.py:26
  90.4 3.0 %collective-permute-done.6 = bf16[2,2,64,2048]{3,2,1,0:T(8,128)(2,1)} collective-permute-done((bf16[2,2,64,2048]{3,2,1,0:T(8,128)(2,1)}, bf16[2,2,64,2048]{3,2,1,0:T(8,128)(2,1)}, u32[]{:S(2)}, u32[]{:S(2)}) %collective-permute-start.6) | collective-permute-done | bytes 1048608 | tf_op jit(solution)/shard_map/ppermute | solution.py:26
  93.4 1.8 %fusion.6 = bf16[2,2,64,2048]{3,2,1,0:T(8,128)(2,1)S(1)} fusion(f32[1,2,2,64,2048]{4,3,2,1,0:T(8,128)} %copy-done, f32[1,2,2,64,2048]{4,3,2,1,0:T(8,128)S(1)} %convolution_bitcast_fusion, bf16[2,2,64,2048]{3,2,1,0:T(8,128)(2,1)} %collective-permute-done.6), kind=kLoop, calls=%fused_computation.22 | loop fusion | flops 2097152 | bytes 6291456 | tf_op jit(solution)/shard_map/add | solution.py:120
  95.5 1.1 fusion.27
  96.5 4.8 %all-to-all-start.1 = ((bf16[8,2,64,512]{3,2,1,0:T(8,128)(2,1)}), bf16[8,2,64,512]{3,2,1,0:T(8,128)(2,1)S(1)}, u32[]{:S(2)}, u32[]{:S(2)}) async-start(bf16[8,2,64,512]{3,2,1,0:T(8,128)(2,1)} %bitcast.39), calls=%async_computation.1 | async-start | bytes 2097152 | tf_op jit(solution)/shard_map/all_to_all | solution.py:30
  101.4 1.4 fusion.41
  102.8 0.5 fusion.51
  103.3 0.2 fusion.32
  103.5 2.2 %collective-permute-start.8 = (bf16[2,8,64,256]{3,2,0,1:T(8,128)(2,1)S(1)}, bf16[2,8,64,256]{3,2,0,1:T(8,128)(2,1)S(1)}, u32[]{:S(2)}, u32[]{:S(2)}) collective-permute-start(bf16[2,8,64,256]{3,2,0,1:T(8,128)(2,1)S(1)} %get-tuple-element.4), channel_id=1, source_target_pairs={{0,64},{64,128},{128,192},{192,256},{256,320},{320,384},{384,448},... | collective-permute-start | bytes 1572872 | tf_op jit(solution)/shard_map/ppermute | solution.py:22
  105.7 4.9 %collective-permute-start.9 = (bf16[2,8,64,256]{3,2,0,1:T(8,128)(2,1)S(1)}, bf16[2,8,64,256]{3,2,0,1:T(8,128)(2,1)S(1)}, u32[]{:S(2)}, u32[]{:S(2)}) collective-permute-start(bf16[2,8,64,256]{3,2,0,1:T(8,128)(2,1)S(1)} %get-tuple-element.5), channel_id=1, source_target_pairs={{0,448},{64,0},{128,64},{192,128},{256,192},{320,256},{384,320},{4... | collective-permute-start | bytes 1572872 | tf_op jit(solution)/shard_map/ppermute | solution.py:22
  110.6 4.6 %collective-permute-start.10 = (bf16[2,4,64,256]{3,2,0,1:T(8,128)(2,1)S(1)}, bf16[2,4,64,256]{3,2,0,1:T(8,128)(2,1)S(1)}, u32[]{:S(2)}, u32[]{:S(2)}) collective-permute-start(bf16[2,4,64,256]{3,2,0,1:T(8,128)(2,1)S(1)} %get-tuple-element.24), channel_id=1, source_target_pairs={{0,128},{64,192},{128,256},{192,320},{256,384},{320,448},{384,0},{... | collective-permute-start | bytes 786440 | tf_op jit(solution)/shard_map/ppermute | solution.py:22
  115.3 3.3 %collective-permute-start.11 = (bf16[2,4,64,256]{3,2,0,1:T(8,128)(2,1)S(1)}, bf16[2,4,64,256]{3,2,0,1:T(8,128)(2,1)S(1)}, u32[]{:S(2)}, u32[]{:S(2)}) collective-permute-start(bf16[2,4,64,256]{3,2,0,1:T(8,128)(2,1)S(1)} %get-tuple-element.25), channel_id=1, source_target_pairs={{0,384},{64,448},{128,0},{192,64},{256,128},{320,192},{384,256},{4... | collective-permute-start | bytes 786440 | tf_op jit(solution)/shard_map/ppermute | solution.py:22
  118.6 9.2 %collective-permute-done.10 = bf16[2,4,64,256]{3,2,0,1:T(8,128)(2,1)S(1)} collective-permute-done((bf16[2,4,64,256]{3,2,0,1:T(8,128)(2,1)S(1)}, bf16[2,4,64,256]{3,2,0,1:T(8,128)(2,1)S(1)}, u32[]{:S(2)}, u32[]{:S(2)}) %collective-permute-start.10) | collective-permute-done | bytes 262176 | tf_op jit(solution)/shard_map/ppermute | solution.py:22
  127.8 7.8 %collective-permute-done.11 = bf16[2,4,64,256]{3,2,0,1:T(8,128)(2,1)S(1)} collective-permute-done((bf16[2,4,64,256]{3,2,0,1:T(8,128)(2,1)S(1)}, bf16[2,4,64,256]{3,2,0,1:T(8,128)(2,1)S(1)}, u32[]{:S(2)}, u32[]{:S(2)}) %collective-permute-start.11) | collective-permute-done | bytes 262176 | tf_op jit(solution)/shard_map/ppermute | solution.py:22
  135.6 1.1 fusion.34
  136.8 6.7 %all-to-all-start.3 = ((bf16[8,2,64,256]{3,2,1,0:T(8,128)(2,1)}), bf16[8,2,64,256]{3,2,1,0:T(8,128)(2,1)S(1)}, u32[]{:S(2)}, u32[]{:S(2)}) async-start(bf16[8,2,64,256]{3,2,1,0:T(8,128)(2,1)} %fusion.34), calls=%async_computation.3 | async-start | bytes 1048576 | tf_op jit(solution)/shard_map/all_to_all | solution.py:30
  143.4 0.1 reduce_sum.50
  143.6 16.0 %all-to-all-done.3 = bf16[8,2,64,256]{3,2,1,0:T(8,128)(2,1)S(1)} async-done(((bf16[8,2,64,256]{3,2,1,0:T(8,128)(2,1)}), bf16[8,2,64,256]{3,2,1,0:T(8,128)(2,1)S(1)}, u32[]{:S(2)}, u32[]{:S(2)}) %all-to-all-start.3) | async-done | bytes 524320 | tf_op jit(solution)/shard_map/all_to_all | solution.py:30
  159.5 0.8 broadcast_in_dim.43
  160.4 4.8 %all-to-all-start.2 = ((bf16[4,2,64,512]{3,2,1,0:T(8,128)(2,1)}), bf16[4,2,64,512]{3,2,1,0:T(8,128)(2,1)S(1)}, u32[]{:S(2)}, u32[]{:S(2)}) async-start(bf16[4,2,64,512]{3,2,1,0:T(8,128)(2,1)} %broadcast_in_dim.43), calls=%async_computation.2 | async-start | bytes 1048576 | tf_op jit(solution)/shard_map/all_to_all | solution.py:30
  165.3 5.1 %collective-permute-start.12 = (bf16[2,2,64,256]{3,2,0,1:T(8,128)(2,1)S(1)}, bf16[2,2,64,256]{3,2,0,1:T(8,128)(2,1)S(1)}, u32[]{:S(2)}, u32[]{:S(2)}) collective-permute-start(bf16[2,2,64,256]{3,2,0,1:T(8,128)(2,1)S(1)} %fusion.40), channel_id=1, source_target_pairs={{0,256},{256,0},{1,257},{257,1},{2,258},{258,2},{3,259},{259,3},{4... | collective-permute-start | bytes 393224 | tf_op jit(solution)/shard_map/ppermute | solution.py:26
  170.3 1.4 all-to-all-done.2
  171.9 0.3 copy.51
  172.2 0.2 copy.64
  172.4 0.2 multiply_reduce_fusion
  172.6 0.1 multiply_convert_fusion.1
  172.8 1.9 %collective-permute-start.7 = (bf16[2,64,2048]{2,1,0:T(8,128)(2,1)S(1)}, bf16[2,64,2048]{2,1,0:T(8,128)(2,1)S(1)}, u32[]{:S(2)}, u32[]{:S(2)}) collective-permute-start(bf16[2,64,2048]{2,1,0:T(8,128)(2,1)S(1)} %pad_maximum_fusion.6), channel_id=1, source_target_pairs={{0,1},{1,0},{2,3},{3,2},{4,5},{5,4},{6,7},{7,6},{8,9},{9,8},{10,11... | collective-permute-start | bytes 1572872 | tf_op jit(solution)/shard_map/ppermute | solution.py:26
  174.8 2.8 %collective-permute-done.12 = bf16[2,2,64,256]{3,2,0,1:T(8,128)(2,1)S(1)} collective-permute-done((bf16[2,2,64,256]{3,2,0,1:T(8,128)(2,1)S(1)}, bf16[2,2,64,256]{3,2,0,1:T(8,128)(2,1)S(1)}, u32[]{:S(2)}, u32[]{:S(2)}) %collective-permute-start.12) | collective-permute-done | bytes 131104 | tf_op jit(solution)/shard_map/ppermute | solution.py:26
  177.6 0.1 copy.55
  177.9 0.7 add.99
  178.6 0.7 bitcast_add_fusion
  179.3 0.2 copy.49
  179.6 0.8 pad_maximum_fusion.8
  180.5 0.8 pad_maximum_fusion.7
  (72 shorter events, 1.4 us)
Async XLA Ops:
  0.6 10.0 %copy-start.4 = (bf16[128,2048]{1,0:T(8,128)(2,1)S(1)}, bf16[128,2048]{1,0:T(8,128)(2,1)}, u32[]{:S(2)}) copy-start(bf16[128,2048]{1,0:T(8,128)(2,1)} %param.9) | copy-start | bytes 1572868
  0.6 10.1 %copy-start.5 = (bf16[128,2048]{1,0:T(8,128)(2,1)S(1)}, bf16[128,2048]{1,0:T(8,128)(2,1)}, u32[]{:S(2)}) copy-start(bf16[128,2048]{1,0:T(8,128)(2,1)} %param.10) | copy-start | bytes 1572868
  0.7 10.1 %copy-start.6 = (bf16[128,2048]{1,0:T(8,128)(2,1)S(1)}, bf16[128,2048]{1,0:T(8,128)(2,1)}, u32[]{:S(2)}) copy-start(bf16[128,2048]{1,0:T(8,128)(2,1)} %param.8) | copy-start | bytes 1572868
  3.6 39.5 %all-to-all-start = ((bf16[8,2,64,256]{3,2,1,0:T(8,128)(2,1)}), bf16[8,2,64,256]{3,2,1,0:T(8,128)(2,1)S(1)}, u32[]{:S(2)}, u32[]{:S(2)}) async-start(bf16[8,2,64,256]{3,2,1,0:T(8,128)(2,1)} %bitcast.9), calls=%async_computation | async-start | bytes 1048576 | tf_op jit(solution)/shard_map/all_to_all | solution.py:30
  11.6 31.5 %copy-start.2 = (bf16[64,2048]{1,0:T(8,128)(2,1)}, bf16[64,2048]{1,0:T(8,128)(2,1)S(1)}, u32[]{:S(2)}) copy-start(bf16[64,2048]{1,0:T(8,128)(2,1)S(1)} %get-tuple-element.32) | copy-start | bytes 786436
  12.6 28.5 %collective-permute-start = (bf16[3,64,2048]{2,1,0:T(8,128)(2,1)}, bf16[3,64,2048]{2,1,0:T(8,128)(2,1)S(1)}, u32[]{:S(2)}, u32[]{:S(2)}) collective-permute-start(bf16[3,64,2048]{2,1,0:T(8,128)(2,1)} %pad_maximum_fusion.5), channel_id=1, source_target_pairs={{0,8},{8,0},{1,9},{9,1},{2,10},{10,2},{3,11},{11,3},{4,12},{12,4},... | collective-permute-start | bytes 2359304 | tf_op jit(solution)/shard_map/ppermute | solution.py:26
  41.1 38.2 %collective-permute-start.1 = (bf16[3,64,2048]{2,1,0:T(8,128)(2,1)S(1)}, bf16[3,64,2048]{2,1,0:T(8,128)(2,1)}, u32[]{:S(2)}, u32[]{:S(2)}) collective-permute-start(bf16[3,64,2048]{2,1,0:T(8,128)(2,1)S(1)} %collective-permute-done), channel_id=1, source_target_pairs={{0,1},{1,0},{2,3},{3,2},{4,5},{5,4},{6,7},{7,6},{8,9},{9,8},{10,11... | collective-permute-start | bytes 2359304 | tf_op jit(solution)/shard_map/ppermute | solution.py:26
  43.0 23.7 %collective-permute-start.2 = (bf16[8,2,64,256]{3,2,1,0:T(8,128)(2,1)S(1)}, bf16[8,2,64,256]{3,2,1,0:T(8,128)(2,1)S(1)}, u32[]{:S(2)}, u32[]{:S(2)}) collective-permute-start(bf16[8,2,64,256]{3,2,1,0:T(8,128)(2,1)S(1)} %all-to-all-done), channel_id=1, source_target_pairs={{0,64},{64,128},{128,192},{192,256},{256,320},{320,384},{384,448},... | collective-permute-start | bytes 1572872 | tf_op jit(solution)/shard_map/ppermute | solution.py:22
  47.4 37.8 %copy-start.7 = (bf16[64,2048]{1,0:T(8,128)(2,1)}, bf16[64,2048]{1,0:T(8,128)(2,1)S(1)}, u32[]{:S(2)}) copy-start(bf16[64,2048]{1,0:T(8,128)(2,1)S(1)} %get-tuple-element.18) | copy-start | bytes 786436
  47.4 26.5 %collective-permute-start.3 = (bf16[8,2,64,256]{3,2,1,0:T(8,128)(2,1)S(1)}, bf16[8,2,64,256]{3,2,1,0:T(8,128)(2,1)S(1)}, u32[]{:S(2)}, u32[]{:S(2)}) collective-permute-start(bf16[8,2,64,256]{3,2,1,0:T(8,128)(2,1)S(1)} %all-to-all-done), channel_id=1, source_target_pairs={{0,448},{64,0},{128,64},{192,128},{256,192},{320,256},{384,320},{4... | collective-permute-start | bytes 1572872 | tf_op jit(solution)/shard_map/ppermute | solution.py:22
  56.0 17.9 %collective-permute-start.4 = (bf16[4,2,64,256]{3,2,1,0:T(8,128)(2,1)S(1)}, bf16[4,2,64,256]{3,2,1,0:T(8,128)(2,1)S(1)}, u32[]{:S(2)}, u32[]{:S(2)}) collective-permute-start(bf16[4,2,64,256]{3,2,1,0:T(8,128)(2,1)S(1)} %get-tuple-element.38), channel_id=1, source_target_pairs={{0,128},{64,192},{128,256},{192,320},{256,384},{320,448},{384,0},{... | collective-permute-start | bytes 786440 | tf_op jit(solution)/shard_map/ppermute | solution.py:22
  58.0 21.1 %collective-permute-start.5 = (bf16[4,2,64,256]{3,2,1,0:T(8,128)(2,1)S(1)}, bf16[4,2,64,256]{3,2,1,0:T(8,128)(2,1)S(1)}, u32[]{:S(2)}, u32[]{:S(2)}) collective-permute-start(bf16[4,2,64,256]{3,2,1,0:T(8,128)(2,1)S(1)} %get-tuple-element.37), channel_id=1, source_target_pairs={{0,384},{64,448},{128,0},{192,64},{256,128},{320,192},{384,256},{4... | collective-permute-start | bytes 786440 | tf_op jit(solution)/shard_map/ppermute | solution.py:22
  79.3 1.8 copy-start.16
  80.5 4.7 %copy-start.9 = (bf16[64,2048]{1,0:T(8,128)(2,1)}, bf16[64,2048]{1,0:T(8,128)(2,1)S(1)}, u32[]{:S(2)}) copy-start(bf16[64,2048]{1,0:T(8,128)(2,1)S(1)} %get-tuple-element.21) | copy-start | bytes 786436
  81.1 84.0 %copy-start.17 = (f32[256]{0:T(256)}, f32[256]{0:T(256)S(1)}, u32[]{:S(2)}) copy-start(f32[256]{0:T(256)S(1)} %add_rsqrt_fusion.1) | copy-start | bytes 3076
  84.4 0.9 copy-start.3
  84.4 1.0 copy-start.11
  85.2 1.2 copy-start.15
  86.9 1.7 copy-start
  88.5 4.9 %collective-permute-start.6 = (bf16[2,2,64,2048]{3,2,1,0:T(8,128)(2,1)}, bf16[2,2,64,2048]{3,2,1,0:T(8,128)(2,1)}, u32[]{:S(2)}, u32[]{:S(2)}) collective-permute-start(bf16[2,2,64,2048]{3,2,1,0:T(8,128)(2,1)} %fusion.14), channel_id=1, source_target_pairs={{0,1},{1,0},{2,3},{3,2},{4,5},{5,4},{6,7},{7,6},{8,9},{9,8},{10,11... | collective-permute-start | bytes 3145736 | tf_op jit(solution)/shard_map/ppermute | solution.py:26
  95.4 5.9 %copy-start.8 = (bf16[64,2048]{1,0:T(8,128)(2,1)S(1)}, bf16[64,2048]{1,0:T(8,128)(2,1)}, u32[]{:S(2)}) copy-start(bf16[64,2048]{1,0:T(8,128)(2,1)} %copy-done.7) | copy-start | bytes 786436
  95.4 5.9 %copy-start.10 = (bf16[64,2048]{1,0:T(8,128)(2,1)S(1)}, bf16[64,2048]{1,0:T(8,128)(2,1)}, u32[]{:S(2)}) copy-start(bf16[64,2048]{1,0:T(8,128)(2,1)} %copy-done.9) | copy-start | bytes 786436
  95.5 5.9 %copy-start.12 = (bf16[64,2048]{1,0:T(8,128)(2,1)S(1)}, bf16[64,2048]{1,0:T(8,128)(2,1)}, u32[]{:S(2)}) copy-start(bf16[64,2048]{1,0:T(8,128)(2,1)} %get-tuple-element.31) | copy-start | bytes 786436
  96.5 40.2 %all-to-all-start.1 = ((bf16[8,2,64,512]{3,2,1,0:T(8,128)(2,1)}), bf16[8,2,64,512]{3,2,1,0:T(8,128)(2,1)S(1)}, u32[]{:S(2)}, u32[]{:S(2)}) async-start(bf16[8,2,64,512]{3,2,1,0:T(8,128)(2,1)} %bitcast.39), calls=%async_computation.1 | async-start | bytes 2097152 | tf_op jit(solution)/shard_map/all_to_all | solution.py:30
  103.5 32.1 %collective-permute-start.8 = (bf16[2,8,64,256]{3,2,0,1:T(8,128)(2,1)S(1)}, bf16[2,8,64,256]{3,2,0,1:T(8,128)(2,1)S(1)}, u32[]{:S(2)}, u32[]{:S(2)}) collective-permute-start(bf16[2,8,64,256]{3,2,0,1:T(8,128)(2,1)S(1)} %get-tuple-element.4), channel_id=1, source_target_pairs={{0,64},{64,128},{128,192},{192,256},{256,320},{320,384},{384,448},... | collective-permute-start | bytes 1572872 | tf_op jit(solution)/shard_map/ppermute | solution.py:22
  105.7 29.9 %collective-permute-start.9 = (bf16[2,8,64,256]{3,2,0,1:T(8,128)(2,1)S(1)}, bf16[2,8,64,256]{3,2,0,1:T(8,128)(2,1)S(1)}, u32[]{:S(2)}, u32[]{:S(2)}) collective-permute-start(bf16[2,8,64,256]{3,2,0,1:T(8,128)(2,1)S(1)} %get-tuple-element.5), channel_id=1, source_target_pairs={{0,448},{64,0},{128,64},{192,128},{256,192},{320,256},{384,320},{4... | collective-permute-start | bytes 1572872 | tf_op jit(solution)/shard_map/ppermute | solution.py:22
  110.6 17.2 %collective-permute-start.10 = (bf16[2,4,64,256]{3,2,0,1:T(8,128)(2,1)S(1)}, bf16[2,4,64,256]{3,2,0,1:T(8,128)(2,1)S(1)}, u32[]{:S(2)}, u32[]{:S(2)}) collective-permute-start(bf16[2,4,64,256]{3,2,0,1:T(8,128)(2,1)S(1)} %get-tuple-element.24), channel_id=1, source_target_pairs={{0,128},{64,192},{128,256},{192,320},{256,384},{320,448},{384,0},{... | collective-permute-start | bytes 786440 | tf_op jit(solution)/shard_map/ppermute | solution.py:22
  115.3 20.3 %collective-permute-start.11 = (bf16[2,4,64,256]{3,2,0,1:T(8,128)(2,1)S(1)}, bf16[2,4,64,256]{3,2,0,1:T(8,128)(2,1)S(1)}, u32[]{:S(2)}, u32[]{:S(2)}) collective-permute-start(bf16[2,4,64,256]{3,2,0,1:T(8,128)(2,1)S(1)} %get-tuple-element.25), channel_id=1, source_target_pairs={{0,384},{64,448},{128,0},{192,64},{256,128},{320,192},{384,256},{4... | collective-permute-start | bytes 786440 | tf_op jit(solution)/shard_map/ppermute | solution.py:22
  136.8 22.8 %all-to-all-start.3 = ((bf16[8,2,64,256]{3,2,1,0:T(8,128)(2,1)}), bf16[8,2,64,256]{3,2,1,0:T(8,128)(2,1)S(1)}, u32[]{:S(2)}, u32[]{:S(2)}) async-start(bf16[8,2,64,256]{3,2,1,0:T(8,128)(2,1)} %fusion.34), calls=%async_computation.3 | async-start | bytes 1048576 | tf_op jit(solution)/shard_map/all_to_all | solution.py:30
  160.4 11.4 %all-to-all-start.2 = ((bf16[4,2,64,512]{3,2,1,0:T(8,128)(2,1)}), bf16[4,2,64,512]{3,2,1,0:T(8,128)(2,1)S(1)}, u32[]{:S(2)}, u32[]{:S(2)}) async-start(bf16[4,2,64,512]{3,2,1,0:T(8,128)(2,1)} %broadcast_in_dim.43), calls=%async_computation.2 | async-start | bytes 1048576 | tf_op jit(solution)/shard_map/all_to_all | solution.py:30
  165.2 7.2 %copy-start.1 = (f32[256,2048]{1,0:T(8,128)S(1)}, f32[256,2048]{1,0:T(8,128)}, u32[]{:S(2)}) copy-start(f32[256,2048]{1,0:T(8,128)} %get-tuple-element.9) | copy-start | bytes 6291460
  165.3 12.3 %collective-permute-start.12 = (bf16[2,2,64,256]{3,2,0,1:T(8,128)(2,1)S(1)}, bf16[2,2,64,256]{3,2,0,1:T(8,128)(2,1)S(1)}, u32[]{:S(2)}, u32[]{:S(2)}) collective-permute-start(bf16[2,2,64,256]{3,2,0,1:T(8,128)(2,1)S(1)} %fusion.40), channel_id=1, source_target_pairs={{0,256},{256,0},{1,257},{257,1},{2,258},{258,2},{3,259},{259,3},{4... | collective-permute-start | bytes 393224 | tf_op jit(solution)/shard_map/ppermute | solution.py:26
  171.9 0.7 slice-start
  172.6 5.3 %copy-start.13 = (f32[64,512]{1,0:T(8,128)S(1)}, f32[64,512]{1,0:T(8,128)}, u32[]{:S(2)}) copy-start(f32[64,512]{1,0:T(8,128)} %param.14) | copy-start | bytes 393220
  172.8 5.8 %copy-start.14 = (f32[512,64]{0,1:T(8,128)S(1)}, f32[512,64]{0,1:T(8,128)}, u32[]{:S(2)}) copy-start(f32[512,64]{0,1:T(8,128)} %param.15) | copy-start | bytes 393220
  172.8 6.7 %collective-permute-start.7 = (bf16[2,64,2048]{2,1,0:T(8,128)(2,1)S(1)}, bf16[2,64,2048]{2,1,0:T(8,128)(2,1)S(1)}, u32[]{:S(2)}, u32[]{:S(2)}) collective-permute-start(bf16[2,64,2048]{2,1,0:T(8,128)(2,1)S(1)} %pad_maximum_fusion.6), channel_id=1, source_target_pairs={{0,1},{1,0},{2,3},{3,2},{4,5},{5,4},{6,7},{7,6},{8,9},{9,8},{10,11... | collective-permute-start | bytes 1572872 | tf_op jit(solution)/shard_map/ppermute | solution.py:26
